TPU v7x, 32 devices: a whole 2x2x4 slice. The times are simulated.
32 devices in a mesh: sp: 8 (over z, y), tp: 4 (over x, core).
Axes of the slice: x: 2, y: 2, z: 4, core: 2. Of those that a mesh axis runs over, the one named last changes fastest.
Arguments:
- queries: bfloat16 [4096, 2048], P('sp', 'tp'), may hold values from -6 to 6
- keys: bfloat16 [4096, 512], P('sp', 'tp'), may hold values from -6 to 6
- values: bfloat16 [4096, 512], P('sp', 'tp'), may hold values from -6 to 6
- residual: bfloat16 [4096, 2048], P(('sp', 'tp')), may hold values from -0.119628906 to 0.119628906
- out_proj: bfloat16 [2048, 2048], replicated, may hold values from -0.125 to 0.125
- query_gain: float32 [128], replicated, may hold values from 0.7 to 7
- key_gain: float32 [128], replicated, may hold values from 0.7 to 7
- norm_gain: float32 [2048], replicated, may hold values from 0.1 to 1.9
- routes: int32 [4096, 4], P(('sp', 'tp')), may hold values from 0 to 31, all different within a row; in each aligned block of 128 rows (0 to 127, 128 to 255, ...) at most 32 rows name the same one
- route_weight: float32 [4096, 4], P(('sp', 'tp')), may hold values from 0.1 to 1
- expert_gate: bfloat16 [32, 2048, 256], P(('sp', 'tp')), may hold values from -0.125 to 0.125
- expert_up: bfloat16 [32, 2048, 256], P(('sp', 'tp')), may hold values from -0.125 to 0.125
- expert_down: bfloat16 [32, 256, 2048], P(('sp', 'tp')), may hold values from -0.375 to 0.375
- shared_gate: bfloat16 [2048, 256], replicated, may hold values from -0.125 to 0.125
- shared_up: bfloat16 [2048, 256], replicated, may hold values from -0.125 to 0.125
- shared_down: bfloat16 [256, 2048], replicated, may hold values from -0.375 to 0.375
Outputs:
- layer_out: bfloat16 [4096, 2048], P(('sp', 'tp'))
Inputs may be any that keep to these rules, and one draw needn't show every extreme that they name: In the rows of one device (aligned blocks of 128 tokens), no expert is named by more than 32 routes; some expert is named by exactly 32 routes of some device; the 4 experts of a token differ.
All inputs are finite; a program needn't handle non-finite values.
Results may differ from a plain program's by a relative error of at most 0.023.
The roundings to bfloat16 on the way count: a program that leaves them out, or rounds other values in their place, can miss the bound.
Values may be sent and summed in bfloat16 or wider, within the bound.
A program may use at most 128 MiB of HBM per device.

v0:
```python
import math
import jax
import jax.numpy as jnp
from jax import lax
from jax.sharding import PartitionSpec as P

HEADS = 16
KV_HEADS = 4
GRID_W = 64
EPS = 1e-06
THETA = 10000.0


def rotate_pairs(block, cosine, sine):
    first, second = jnp.split(block, 2, axis=-1)
    return jnp.concatenate(
        [first * cosine - second * sine, second * cosine + first * sine], axis=-1
    )


def normed_rotary(source, gain, heads, offset):
    count = source.shape[0]
    width = gain.shape[0]
    values_f = source.astype(jnp.float32).reshape(count, heads, width)
    values_f = (
        values_f * lax.rsqrt(jnp.mean(values_f * values_f, axis=-1, keepdims=True) + EPS) * gain
    )
    position = offset + jnp.arange(count, dtype=jnp.int32)
    grid_row = (position // GRID_W).astype(jnp.float32)
    grid_col = (position % GRID_W).astype(jnp.float32)
    quarter = width // 4
    inverse = jnp.power(THETA, -4.0 * jnp.arange(quarter, dtype=jnp.float32) / width)
    row_angle = (grid_row[:, None] * inverse[None, :])[:, None, :]
    col_angle = (grid_col[:, None] * inverse[None, :])[:, None, :]
    row_half, col_half = jnp.split(values_f, 2, axis=-1)
    turned = jnp.concatenate(
        [
            rotate_pairs(row_half, jnp.cos(row_angle), jnp.sin(row_angle)),
            rotate_pairs(col_half, jnp.cos(col_angle), jnp.sin(col_angle)),
        ],
        axis=-1,
    )
    return turned.reshape(count, heads * width).astype(jnp.bfloat16)


def expert_apply(arrived, expert_gate, expert_up, expert_down):
    sources, slots, width = arrived.shape
    local = expert_gate.shape[0]
    grouped = arrived.reshape(sources // local, local, slots, width)
    gate_part = jnp.einsum(
        "sech,ehf->secf", grouped, expert_gate, preferred_element_type=jnp.float32
    )
    up_part = jnp.einsum("sech,ehf->secf", grouped, expert_up, preferred_element_type=jnp.float32)
    hidden_e = (jax.nn.silu(gate_part) * up_part).astype(jnp.bfloat16)
    result = jnp.einsum("secf,efh->sech", hidden_e, expert_down, preferred_element_type=jnp.float32)
    return result.astype(jnp.bfloat16).reshape(sources, slots, width)


def body(
    queries,
    keys,
    values,
    residual,
    out_proj,
    query_gain,
    key_gain,
    norm_gain,
    routes,
    route_weight,
    expert_gate,
    expert_up,
    expert_down,
    shared_gate,
    shared_up,
    shared_down,
):
    tok_local = queries.shape[0]
    width = query_gain.shape[0]
    group = HEADS // KV_HEADS
    kv_local = keys.shape[1] // width
    scale = 1.0 / math.sqrt(width)
    offset = lax.axis_index("sp") * tok_local
    q_rot = normed_rotary(queries, query_gain, kv_local * group, offset)
    k_rot = normed_rotary(keys, key_gain, kv_local, offset)
    query_3d = q_rot.reshape(tok_local, kv_local, group, width).transpose(1, 2, 0, 3)
    query_3d = query_3d.reshape(kv_local, group * tok_local, width)
    start_state = (
        jnp.full((kv_local, group * tok_local), -jnp.inf, jnp.float32),
        jnp.zeros((kv_local, group * tok_local), jnp.float32),
        jnp.zeros((kv_local, group * tok_local, width), jnp.float32),
    )
    key_piece = lax.all_gather(k_rot, "sp", axis=0, tiled=True)
    value_piece = lax.all_gather(values, "sp", axis=0, tiled=True)
    count = key_piece.shape[0]
    block = math.gcd(count, 512)

    def one_block(index_block, state):
        running_max, running_sum, accum = state
        key_rows = lax.dynamic_slice_in_dim(key_piece, index_block * block, block, 0)
        value_rows = lax.dynamic_slice_in_dim(value_piece, index_block * block, block, 0)
        key_3d = key_rows.reshape(block, kv_local, width)
        value_3d = value_rows.reshape(block, kv_local, width)
        scores = (
            jnp.einsum("gqd,kgd->gqk", query_3d, key_3d, preferred_element_type=jnp.float32) * scale
        )
        new_max = jnp.maximum(running_max, jnp.max(scores, axis=-1))
        weights = jnp.exp(scores - new_max[..., None])
        factor = jnp.exp(running_max - new_max)
        new_sum = running_sum * factor + jnp.sum(weights, axis=-1)
        added = jnp.einsum(
            "gqk,kgd->gqd",
            weights.astype(jnp.bfloat16),
            value_3d,
            preferred_element_type=jnp.float32,
        )
        return (new_max, new_sum, accum * factor[..., None] + added)

    final_max, final_sum, final_acc = lax.fori_loop(0, count // block, one_block, start_state)
    attn_local = (final_acc / final_sum[..., None]).astype(jnp.bfloat16)
    attn_local = attn_local.reshape(kv_local, group, tok_local, width).transpose(2, 0, 1, 3)
    attn_local = attn_local.reshape(tok_local, kv_local * group * width)
    all_heads = lax.all_to_all(attn_local, "tp", split_axis=0, concat_axis=1, tiled=True)
    projected = jnp.dot(all_heads, out_proj, preferred_element_type=jnp.float32)
    hidden1 = (residual.astype(jnp.float32) + projected).astype(jnp.bfloat16)
    hidden_f = hidden1.astype(jnp.float32)
    normed = (
        hidden_f
        * lax.rsqrt(jnp.mean(hidden_f * hidden_f, axis=-1, keepdims=True) + EPS)
        * norm_gain
    ).astype(jnp.bfloat16)
    rows_local = normed.shape[0]
    top_count = routes.shape[1]
    pair_count = rows_local * top_count
    expert_total = expert_gate.shape[0] * lax.axis_size("sp") * lax.axis_size("tp")
    capacity = max(2, 2 * rows_local * top_count // expert_total)
    flat_routes = routes.reshape(pair_count)
    one_hot = (flat_routes[:, None] == jnp.arange(expert_total, dtype=jnp.int32)[None, :]).astype(
        jnp.float32
    )
    lower = (jnp.arange(pair_count)[:, None] >= jnp.arange(pair_count)[None, :]).astype(jnp.float32)
    running_count = jnp.dot(lower, one_hot, precision=lax.Precision.HIGHEST)
    slot_place = (jnp.sum(running_count * one_hot, axis=1) - 1.0).astype(jnp.int32)
    slot_index = flat_routes * capacity + slot_place
    slot_total = expert_total * capacity
    placement = (jnp.arange(slot_total, dtype=jnp.int32)[:, None] == slot_index[None, :]).astype(
        jnp.bfloat16
    )
    placement = jnp.sum(placement.reshape(slot_total, rows_local, top_count), axis=2)
    send_rows = jnp.dot(placement, normed, preferred_element_type=jnp.float32).astype(jnp.bfloat16)
    send_rows = send_rows.reshape(expert_total, capacity, normed.shape[1])
    shared_hidden = (
        jax.nn.silu(jnp.dot(normed, shared_gate, preferred_element_type=jnp.float32))
        * jnp.dot(normed, shared_up, preferred_element_type=jnp.float32)
    ).astype(jnp.bfloat16)
    shared_out = jnp.dot(shared_hidden, shared_down, preferred_element_type=jnp.float32)
    processed = expert_apply(
        lax.all_to_all(send_rows, ("sp", "tp"), split_axis=0, concat_axis=0, tiled=True),
        expert_gate,
        expert_up,
        expert_down,
    )
    returned = lax.all_to_all(processed, ("sp", "tp"), split_axis=0, concat_axis=0, tiled=True)
    returned = returned.reshape(slot_total, normed.shape[1])
    routed = (
        returned[slot_index].reshape(rows_local, top_count, normed.shape[1]).astype(jnp.float32)
    )
    mixed = jnp.einsum("tk,tkd->td", route_weight, routed) + shared_out
    return (hidden_f + mixed).astype(jnp.bfloat16)


def solution(mesh):
    placed = (
        P("sp", "tp"),
        P("sp", "tp"),
        P("sp", "tp"),
        P(("sp", "tp"), None),
        P(),
        P(),
        P(),
        P(),
        P(("sp", "tp"), None),
        P(("sp", "tp"), None),
        P(("sp", "tp"), None, None),
        P(("sp", "tp"), None, None),
        P(("sp", "tp"), None, None),
        P(),
        P(),
        P(),
    )
    return jax.shard_map(
        body, mesh=mesh, in_specs=placed, out_specs=P(("sp", "tp"), None), check_vma=False
    )
```

profile of v0, /device:TPU:0, one launch (start us, length us, event | category | flops | bytes accessed | tf_op | source)
XLA Modules:
  0.0 420.8 jit_solution(3090994777994951920)
XLA Ops:
  6.6 1.1 copy.35
  7.7 0.7 fusion.43
  10.5 1.4 reshape.480
  12.6 1.9 multiply_cosine_fusion.1
  15.2 1.8 fusion.37
  17.0 1.6 maximum_bitcast_fusion
  19.2 32.9 %all-gather.6.cloned.1.call-done = bf16[4096,1,128]{0,2,1:T(8,128)(2,1)} async-done(((bf16[512,1,128]{0,2,1:T(8,128)(2,1)}), bf16[4096,1,128]{0,2,1:T(8,128)(2,1)}) %all-gather.6.cloned.1.call-update) | async-done | bytes 1048592 | tf_op jit(solution)/shard_map/all_gather | solution.py:92
  52.1 41.4 %all-gather.4.cloned.1.call-done = bf16[4096,128]{1,0:T(8,128)(2,1)} async-done(((bf16[512,128]{1,0:T(8,128)(2,1)}), bf16[4096,128]{1,0:T(8,128)(2,1)}) %all-gather.4.cloned.1.call-update) | async-done | bytes 1048592 | tf_op jit(solution)/shard_map/all_gather | solution.py:93
  93.6 73.7 %while.18 = (s32[]{:T(128)}, f32[1,2048]{1,0:T(1,128)S(1)}, f32[1,2048]{1,0:T(1,128)S(1)}, f32[1,2048,128]{2,1,0:T(8,128)S(1)}, bf16[4096,128]{0,1:T(8,128)(2,1)...) while((s32[]{:T(128)}, f32[1,2048]{1,0:T(1,128)S(1)}, ...), condition=%wide.region_5.6_spmd.clone, body=%wide.region_2.5_spmd.clone.sunk | while | flops 546056192 | bytes 32374984 | solution.py:118
  93.6 3.6 multiply_reduce_fusion.4
  97.2 3.0 fusion.96
  100.6 2.1 fusion.98
  102.8 3.6 multiply_reduce_fusion.4
  106.4 3.0 fusion.96
  109.8 2.1 fusion.98
  112.0 3.6 multiply_reduce_fusion.4
  115.6 3.0 fusion.96
  119.0 2.1 fusion.98
  121.2 3.6 multiply_reduce_fusion.4
  124.8 3.0 fusion.96
  128.3 2.1 fusion.98
  130.4 3.6 multiply_reduce_fusion.4
  134.1 3.0 fusion.96
  137.5 2.1 fusion.98
  139.7 3.6 multiply_reduce_fusion.4
  143.3 3.0 fusion.96
  146.7 2.1 fusion.98
  148.9 3.6 multiply_reduce_fusion.4
  152.5 3.0 fusion.96
  155.9 2.1 fusion.98
  158.1 3.6 multiply_reduce_fusion.4
  161.7 3.0 fusion.96
  165.2 2.1 fusion.98
  168.1 1.0 all_to_all.20
  169.1 3.7 all-to-all-start
  173.2 8.1 %all-to-all-done = bf16[4,128,512]{2,1,0:T(8,128)(2,1)S(1)} async-done(((bf16[4,128,512]{2,1,0:T(8,128)(2,1)}), bf16[4,128,512]{2,1,0:T(8,128)(2,1)S(1)}, u32[]{:S(2)}, u32[]{:S(2)}) %all-to-all-start) | async-done | bytes 524320 | tf_op jit(solution)/shard_map/all_to_all | solution.py:122
  181.6 4.7 %multiply_reduce_fusion.1 = (f32[128]{0:T(128)S(1)}, f32[128,2048]{1,0:T(8,128)S(1)}) fusion(bf16[128,2048]{0,1:T(8,128)(2,1)S(1)} %bitcast.106, bf16[2048,2048]{1,0:T(8,128)(2,1)} %param.22, bf16[128,2048]{1,0:T(8,128)(2,1)S(1)} %copy-done.5), kind=kOutput, calls=%fused_computation.52 | convolution fusion | flops 1075314560 | bytes 10486272 | tf_op jit(solution)/shard_map/dot_general | solution.py:123
  186.4 1.3 convolution_convert_fusion.1
  187.8 95.8 %all_to_all.29 = bf16[32,32,2048]{2,1,0:T(8,128)(2,1)S(1)} all-to-all(bf16[32,32,2048]{2,1,0:T(8,128)(2,1)S(1)} %bitcast.103), channel_id=1, replica_groups=mesh['sp'=8,'tp'=4] {'sp','tp'}, dimensions={0} | all-to-all | bytes 8388608 | tf_op jit(solution)/shard_map/all_to_all | solution.py:157
  283.6 2.0 copy-done.2
  285.6 2.3 convolution_bitcast_fusion.2
  287.9 9.1 %convolution_convert_fusion = bf16[32,32,2048]{2,1,0:T(8,128)(2,1)} fusion(bf16[32,32,2048]{2,1,0:T(8,128)(2,1)} %copy-done.2, bf16[1,256,2048]{2,1,0:T(8,128)(2,1)S(1)} %copy-done, bf16[1,2048,256]{2,1,0:T(8,128)(2,1)} %param.29, f32[32,1,32,256]{3,2,0,1:T(8,128)} %convolution_bitcast_fusion.2), kind=kOutput, calls=%fused_computation.23 | convolution fusion | flops 2151153664 | bytes 11534336 | tf_op jit(solution)/shard_map/secf,efh->sech/dot_general | solution.py:55
  297.0 4.0 all-to-all-start.2
  301.7 93.0 %all-to-all-done.2 = bf16[32,32,2048]{2,1,0:T(8,128)(2,1)} async-done(((bf16[32,32,2048]{2,1,0:T(8,128)(2,1)}), bf16[32,32,2048]{2,1,0:T(8,128)(2,1)}, u32[]{:S(2)}, u32[]{:S(2)}) %all-to-all-start.2) | async-done | bytes 4194336 | tf_op jit(solution)/shard_map/all_to_all | solution.py:162
  394.7 8.0 %gather_fusion = bf16[512,2048]{1,0:T(8,128)(2,1)} fusion(bf16[1024,2048]{1,0:T(8,128)(2,1)} %bitcast.29, s32[1024]{0:T(1024)S(1)} %pad_clamp_fusion), kind=kCustom, calls=%fused_computation | custom fusion | bytes 4196352 | tf_op jit(solution)/shard_map/gather | solution.py:165
  402.7 4.2 reshape.478
  406.9 3.8 fusion.76
  410.7 3.3 fusion.19
  (93 shorter events, 9.3 us)
Async XLA Ops:
  6.5 281.3 %copy-start = (bf16[1,256,2048]{2,1,0:T(8,128)(2,1)S(1)}, bf16[1,256,2048]{2,1,0:T(8,128)(2,1)}, u32[]{:S(2)}) copy-start(bf16[1,256,2048]{2,1,0:T(8,128)(2,1)} %param.30) | copy-start | bytes 3145732
  6.5 7.9 %copy-start.9 = (f32[128]{0:T(128)S(1)}, f32[128]{0:T(128)}, u32[]{:S(2)}) copy-start(f32[128]{0:T(128)} %param.23) | copy-start | bytes 1540
  6.5 45.6 %all-gather.6.cloned.1.call-start = ((), (), s32[]{:S(2)}) async-start(), calls=%async_computation.4 | async-start | bytes 1179648 | tf_op jit(solution)/shard_map/all_gather | solution.py:92
  9.7 83.8 %all-gather.4.cloned.1.call-start = ((), (), s32[]{:S(2)}) async-start(), calls=%async_computation.3 | async-start | bytes 1179648 | tf_op jit(solution)/shard_map/all_gather | solution.py:93
  15.2 3.5 copy-start.7
  97.2 3.4 copy-start.1
  106.4 3.4 copy-start.1
  115.6 3.4 copy-start.1
  124.8 3.4 copy-start.1
  134.0 3.4 copy-start.1
  143.3 3.4 copy-start.1
  152.5 3.4 copy-start.1
  161.7 3.4 copy-start.1
  167.3 14.3 %copy-start.5 = (bf16[128,2048]{1,0:T(8,128)(2,1)S(1)}, bf16[128,2048]{1,0:T(8,128)(2,1)}, u32[]{:S(2)}) copy-start(bf16[128,2048]{1,0:T(8,128)(2,1)} %param.21) | copy-start | bytes 1572868
  169.1 12.3 %all-to-all-start = ((bf16[4,128,512]{2,1,0:T(8,128)(2,1)}), bf16[4,128,512]{2,1,0:T(8,128)(2,1)S(1)}, u32[]{:S(2)}, u32[]{:S(2)}) async-start(bf16[4,128,512]{2,1,0:T(8,128)(2,1)} %all_to_all.20), calls=%async_computation | async-start | bytes 1048576 | tf_op jit(solution)/shard_map/all_to_all | solution.py:122
  181.6 4.8 %copy-start.6 = (f32[2048]{0:T(1024)S(1)}, f32[2048]{0:T(1024)}, u32[]{:S(2)}) copy-start(f32[2048]{0:T(1024)} %param.25) | copy-start | bytes 24580
  187.7 97.8 %copy-start.10 = (bf16[1,2048,256]{2,1,0:T(8,128)(2,1)S(1)}, bf16[1,2048,256]{2,1,0:T(8,128)(2,1)}, u32[]{:S(2)}) copy-start(bf16[1,2048,256]{2,1,0:T(8,128)(2,1)} %param.28) | copy-start | bytes 3145732
  283.6 2.0 copy-start.2
  297.0 4.1 copy-start.8
  297.0 4.3 %copy-start.4 = (bf16[2048,256]{1,0:T(8,128)(2,1)S(1)}, bf16[2048,256]{1,0:T(8,128)(2,1)}, u32[]{:S(2)}) copy-start(bf16[2048,256]{1,0:T(8,128)(2,1)} %param.31) | copy-start | bytes 3145732
  297.0 97.7 %all-to-all-start.2 = ((bf16[32,32,2048]{2,1,0:T(8,128)(2,1)}), bf16[32,32,2048]{2,1,0:T(8,128)(2,1)}, u32[]{:S(2)}, u32[]{:S(2)}) async-start(bf16[32,32,2048]{2,1,0:T(8,128)(2,1)} %convolution_convert_fusion), calls=%async_computation.2 | async-start | bytes 8388608 | tf_op jit(solution)/shard_map/all_to_all | solution.py:162
  402.7 8.0 %copy-start.3 = (bf16[256,2048]{1,0:T(8,128)(2,1)S(1)}, bf16[256,2048]{1,0:T(8,128)(2,1)}, u32[]{:S(2)}) copy-start(bf16[256,2048]{1,0:T(8,128)(2,1)} %param.33) | copy-start | bytes 3145732
Sparse Core Ops, SparseCore 0:
  9.9 42.2 all-gather.5
  54.2 39.2 all-gather.3
where the time goes:
time: 422 us; the launch traced here: 421 us
  waiting for transfers between devices  176 us (42%)
  blocking collectives  95.8 us (23%)
  matrix products  71 us (17%)
  other arithmetic  34.1 us (8%)
  local copies, waits for them, and re-layouts  21.8 us (5%)
  between operations  13.7 us (3%)
  starting transfers between devices  7.71 us (2%)
    all_to_all x1, blocking collectives, body(): lax.all_to_all(send_rows, ('sp', 'tp'), split_axis=0, concat_axis=0, tile...  95.8 us
    all_to_all x1, waiting for transfers between devices, body(): lax.all_to_all(processed, ('sp', 'tp'), split_axis=0, concat_axis=0, tile...  93 us
    all_gather x1, waiting for transfers between devices, body(): value_piece = lax.all_gather(values, 'sp', axis=0, tiled=True)  41.4 us
    all_gather x1, waiting for transfers between devices, body(): key_piece = lax.all_gather(k_rot, 'sp', axis=0, tiled=True)  32.9 us
    dot_general x8, matrix products, one_block(): jnp.einsum('gqd,kgd->gqk', query_3d, key_3d, preferred_element_type=jnp.f...  28.8 us
    reduce_sum x8, other arithmetic, one_block(): new_sum = running_sum * factor + jnp.sum(weights, axis=-1)  24.4 us
    dot_general x8, matrix products, one_block(): jnp.einsum('gqk,kgd->gqd', weights.astype(jnp.bfloat16), value_3d, prefer...  17.1 us
    dot_general x1, matrix products, expert_apply(): jnp.einsum('secf,efh->sech', hidden_e, expert_down, preferred_element_typ...  9.08 us
  transfers between devices with their start and end apart: 4, of which 4 were waited for; matrix products, arithmetic and copies ran while one was open for 2% of the time, Pallas kernels for 0%

commit v1 on v0

--- a/solution.py
+++ b/solution.py
@@ -89,7 +89,12 @@
         jnp.zeros((kv_local, group * tok_local), jnp.float32),
         jnp.zeros((kv_local, group * tok_local, width), jnp.float32),
     )
-    key_piece = lax.all_gather(k_rot, "sp", axis=0, tiled=True)
+    ring = [k_rot]
+    for hop in range(7):
+        ring.append(lax.ppermute(ring[-1], "sp", [(dev, (dev + 1) % 8) for dev in range(8)]))
+    key_piece = jnp.roll(
+        jnp.concatenate(ring[::-1], axis=0), (lax.axis_index("sp") + 1) * ring[0].shape[0], axis=0
+    )
     value_piece = lax.all_gather(values, "sp", axis=0, tiled=True)
     count = key_piece.shape[0]
     block = math.gcd(count, 512)

time: 422 us -> 404 us (0.957)
  waiting for transfers between devices: 176 us -> 147 us
  local copies, waits for them, and re-layouts: 21.8 us -> 30.6 us
    ppermute x0 -> x7, waiting for transfers between devices: none -> 45.3 us  [body(): lax.ppermute(ring[-1], 'sp', [(dev, (dev + 1) % 8) for dev in range(8)])]
    all_gather x1, waiting for transfers between devices: 41.4 us -> 0.01 us  [body(): value_piece = lax.all_gather(values, 'sp', axis=0, tiled=True)]
    all_gather x1 -> x0, waiting for transfers between devices: 32.9 us -> none  [body(): key_piece = lax.all_gather(k_rot, 'sp', axis=0, tiled=True)]
    unnamed x23 -> x59, local copies, waits for them, and re-layouts: 3.38 us -> 11.2 us
  transfers between devices with their start and end apart: 4 -> 10, of which waited for: 4 -> 9; matrix products, arithmetic and copies ran while one was open for 2% -> 5% of each run, Pallas kernels for 0% -> 0%
where the time goes in v1:
time: 404 us; the launch traced here: 403 us
  waiting for transfers between devices  147 us (36%)
  blocking collectives  95.5 us (24%)
  matrix products  71.7 us (18%)
  other arithmetic  34.3 us (8%)
  local copies, waits for them, and re-layouts  30.6 us (8%)
  between operations  14 us (3%)
  starting transfers between devices  10.3 us (3%)
    all_to_all x1, blocking collectives, body(): lax.all_to_all(send_rows, ('sp', 'tp'), split_axis=0, concat_axis=0, tile...  95.5 us
    all_to_all x1, waiting for transfers between devices, body(): lax.all_to_all(processed, ('sp', 'tp'), split_axis=0, concat_axis=0, tile...  93 us
    ppermute x7, waiting for transfers between devices, body(): lax.ppermute(ring[-1], 'sp', [(dev, (dev + 1) % 8) for dev in range(8)])  45.3 us
    dot_general x8, matrix products, one_block(): jnp.einsum('gqd,kgd->gqk', query_3d, key_3d, preferred_element_type=jnp.f...  28.7 us
    reduce_sum x8, other arithmetic, one_block(): new_sum = running_sum * factor + jnp.sum(weights, axis=-1)  24.4 us
    dot_general x8, matrix products, one_block(): jnp.einsum('gqk,kgd->gqd', weights.astype(jnp.bfloat16), value_3d, prefer...  17.1 us
    unnamed x59, local copies, waits for them, and re-layouts  11.2 us
    dot_general x1, matrix products, expert_apply(): jnp.einsum('secf,efh->sech', hidden_e, expert_down, preferred_element_typ...  9.08 us
  transfers between devices with their start and end apart: 10, of which 9 were waited for; matrix products, arithmetic and copies ran while one was open for 5% of the time, Pallas kernels for 0%

profile of v1, /device:TPU:0, one launch (start us, length us, event | category | flops | bytes accessed | tf_op | source)
XLA Modules:
  0.0 403.3 jit_solution(7338043587615326091)
XLA Ops:
  9.7 3.0 collective-permute-start
  14.2 5.1 %collective-permute-done = bf16[512,128]{0,1:T(8,128)(2,1)S(1)} collective-permute-done((bf16[512,128]{0,1:T(8,128)(2,1)S(1)}, bf16[512,128]{0,1:T(8,128)(2,1)S(1)}, u32[]{:S(2)}, u32[]{:S(2)}) %collective-permute-start) | collective-permute-done | bytes 131104 | tf_op jit(solution)/shard_map/ppermute | solution.py:94
  19.9 7.5 %collective-permute-done.1 = bf16[512,128]{0,1:T(8,128)(2,1)S(1)} collective-permute-done((bf16[512,128]{0,1:T(8,128)(2,1)S(1)}, bf16[512,128]{0,1:T(8,128)(2,1)S(1)}, u32[]{:S(2)}, u32[]{:S(2)}) %collective-permute-start.1) | collective-permute-done | bytes 131104 | tf_op jit(solution)/shard_map/ppermute | solution.py:94
  27.5 8.3 %collective-permute-done.2 = bf16[512,128]{0,1:T(8,128)(2,1)S(1)} collective-permute-done((bf16[512,128]{0,1:T(8,128)(2,1)S(1)}, bf16[512,128]{0,1:T(8,128)(2,1)S(1)}, u32[]{:S(2)}, u32[]{:S(2)}) %collective-permute-start.2) | collective-permute-done | bytes 131104 | tf_op jit(solution)/shard_map/ppermute | solution.py:94
  36.5 7.1 %collective-permute-done.3 = bf16[512,128]{0,1:T(8,128)(2,1)S(1)} collective-permute-done((bf16[512,128]{0,1:T(8,128)(2,1)S(1)}, bf16[512,128]{0,1:T(8,128)(2,1)S(1)}, u32[]{:S(2)}, u32[]{:S(2)}) %collective-permute-start.3) | collective-permute-done | bytes 131104 | tf_op jit(solution)/shard_map/ppermute | solution.py:94
  43.6 1.9 multiply_cosine_fusion.1
  45.5 6.9 %collective-permute-done.4 = bf16[512,128]{0,1:T(8,128)(2,1)S(1)} collective-permute-done((bf16[512,128]{0,1:T(8,128)(2,1)S(1)}, bf16[512,128]{0,1:T(8,128)(2,1)S(1)}, u32[]{:S(2)}, u32[]{:S(2)}) %collective-permute-start.4) | collective-permute-done | bytes 131104 | tf_op jit(solution)/shard_map/ppermute | solution.py:94
  52.3 1.8 fusion.37
  54.2 6.0 %collective-permute-done.5 = bf16[512,128]{0,1:T(8,128)(2,1)} collective-permute-done((bf16[512,128]{0,1:T(8,128)(2,1)S(1)}, bf16[512,128]{0,1:T(8,128)(2,1)}, u32[]{:S(2)}, u32[]{:S(2)}) %collective-permute-start.5) | collective-permute-done | bytes 131104 | tf_op jit(solution)/shard_map/ppermute | solution.py:94
  63.7 4.4 %collective-permute-done.6 = bf16[512,128]{0,1:T(8,128)(2,1)} collective-permute-done((bf16[512,128]{0,1:T(8,128)(2,1)}, bf16[512,128]{0,1:T(8,128)(2,1)}, u32[]{:S(2)}, u32[]{:S(2)}) %collective-permute-start.6) | collective-permute-done | bytes 131104 | tf_op jit(solution)/shard_map/ppermute | solution.py:94
  76.6 73.8 %while.18 = (s32[]{:T(128)}, f32[1,2048]{1,0:T(1,128)S(1)}, f32[1,2048]{1,0:T(1,128)S(1)}, f32[1,2048,128]{2,1,0:T(8,128)S(1)}, bf16[4096,128]{0,1:T(8,128)(2,1)...) while((s32[]{:T(128)}, f32[1,2048]{1,0:T(1,128)S(1)}, ...), condition=%wide.region_5.6_spmd.clone, body=%wide.region_2.5_spmd.clone.sunk | while | flops 546056192 | bytes 32374992 | solution.py:123
  76.6 3.6 multiply_reduce_fusion.4
  80.2 3.0 fusion.96
  83.7 2.1 fusion.98
  85.8 3.6 multiply_reduce_fusion.4
  89.5 3.0 fusion.96
  92.9 2.1 fusion.98
  95.1 3.6 multiply_reduce_fusion.4
  98.7 3.0 fusion.96
  102.1 2.1 fusion.98
  104.3 3.6 multiply_reduce_fusion.4
  107.9 3.0 fusion.96
  111.3 2.1 fusion.98
  113.5 3.6 multiply_reduce_fusion.4
  117.1 3.0 fusion.96
  120.6 2.1 fusion.98
  122.7 3.6 multiply_reduce_fusion.4
  126.3 3.0 fusion.96
  129.8 2.1 fusion.98
  132.0 3.6 multiply_reduce_fusion.4
  135.6 3.0 fusion.96
  139.0 2.1 fusion.98
  141.2 3.6 multiply_reduce_fusion.4
  144.8 3.0 fusion.96
  148.2 2.1 fusion.98
  152.2 3.5 all-to-all-start
  156.1 8.3 %all-to-all-done = bf16[4,128,512]{2,1,0:T(8,128)(2,1)S(1)} async-done(((bf16[4,128,512]{2,1,0:T(8,128)(2,1)}), bf16[4,128,512]{2,1,0:T(8,128)(2,1)S(1)}, u32[]{:S(2)}, u32[]{:S(2)}) %all-to-all-start) | async-done | bytes 524320 | tf_op jit(solution)/shard_map/all_to_all | solution.py:127
  164.7 4.7 %multiply_reduce_fusion.1 = (f32[128]{0:T(128)S(1)}, f32[128,2048]{1,0:T(8,128)S(1)}) fusion(bf16[128,2048]{0,1:T(8,128)(2,1)S(1)} %bitcast.111, bf16[2048,2048]{1,0:T(8,128)(2,1)} %param.22, bf16[128,2048]{1,0:T(8,128)(2,1)S(1)} %copy-done.5), kind=kOutput, calls=%fused_computation.52 | convolution fusion | flops 1075314560 | bytes 10486272 | tf_op jit(solution)/shard_map/dot_general | solution.py:128
  170.8 95.5 %all_to_all.29 = bf16[32,32,2048]{2,1,0:T(8,128)(2,1)S(1)} all-to-all(bf16[32,32,2048]{2,1,0:T(8,128)(2,1)S(1)} %bitcast.108), channel_id=1, replica_groups=mesh['sp'=8,'tp'=4] {'sp','tp'}, dimensions={0} | all-to-all | bytes 8388608 | tf_op jit(solution)/shard_map/all_to_all | solution.py:162
  266.3 2.0 copy-done.2
  268.3 2.3 convolution_bitcast_fusion.2
  270.7 9.1 %convolution_convert_fusion = bf16[32,32,2048]{2,1,0:T(8,128)(2,1)} fusion(bf16[32,32,2048]{2,1,0:T(8,128)(2,1)} %copy-done.2, bf16[1,256,2048]{2,1,0:T(8,128)(2,1)S(1)} %copy-done, bf16[1,2048,256]{2,1,0:T(8,128)(2,1)} %param.29, f32[32,1,32,256]{3,2,0,1:T(8,128)} %convolution_bitcast_fusion.2), kind=kOutput, calls=%fused_computation.23 | convolution fusion | flops 2151153664 | bytes 11534336 | tf_op jit(solution)/shard_map/secf,efh->sech/dot_general | solution.py:55
  279.7 3.7 all-to-all-start.2
  284.1 93.0 %all-to-all-done.2 = bf16[32,32,2048]{2,1,0:T(8,128)(2,1)} async-done(((bf16[32,32,2048]{2,1,0:T(8,128)(2,1)}), bf16[32,32,2048]{2,1,0:T(8,128)(2,1)}, u32[]{:S(2)}, u32[]{:S(2)}) %all-to-all-start.2) | async-done | bytes 4194336 | tf_op jit(solution)/shard_map/all_to_all | solution.py:167
  377.2 8.0 %gather_fusion = bf16[512,2048]{1,0:T(8,128)(2,1)} fusion(bf16[1024,2048]{1,0:T(8,128)(2,1)} %bitcast.29, s32[1024]{0:T(1024)S(1)} %pad_clamp_fusion), kind=kCustom, calls=%fused_computation | custom fusion | bytes 4196352 | tf_op jit(solution)/shard_map/gather | solution.py:170
  385.1 4.1 %reshape.478 = bf16[128,4,2048]{2,1,0:T(4,128)(2,1)} reshape(bf16[512,2048]{1,0:T(8,128)(2,1)} %gather_fusion) | data formatting | bytes 4194304 | tf_op jit(solution)/shard_map/reshape | solution.py:170
  389.2 3.9 fusion.76
  393.1 3.3 fusion.19
  (143 shorter events, 25.3 us)
Async XLA Ops:
  6.5 264.1 %copy-start = (bf16[1,256,2048]{2,1,0:T(8,128)(2,1)S(1)}, bf16[1,256,2048]{2,1,0:T(8,128)(2,1)}, u32[]{:S(2)}) copy-start(bf16[1,256,2048]{2,1,0:T(8,128)(2,1)} %param.30) | copy-start | bytes 3145732
  6.5 70.1 %all-gather.2.cloned.1.call-start = ((), (), s32[]{:S(2)}) async-start(), calls=%async_computation.3 | async-start | bytes 1179648 | tf_op jit(solution)/shard_map/all_gather | solution.py:98
  8.5 27.3 %copy-start.20 = (f32[128]{0:T(128)S(1)}, f32[128]{0:T(128)}, u32[]{:S(2)}) copy-start(f32[128]{0:T(128)} %param.23) | copy-start | bytes 1540
  9.1 0.6 copy-start.9
  9.1 0.6 copy-start.11
  9.1 0.6 copy-start.13
  9.1 0.6 copy-start.15
  9.7 9.6 %collective-permute-start = (bf16[512,128]{0,1:T(8,128)(2,1)S(1)}, bf16[512,128]{0,1:T(8,128)(2,1)S(1)}, u32[]{:S(2)}, u32[]{:S(2)}) collective-permute-start(bf16[512,128]{0,1:T(8,128)(2,1)S(1)} %maximum_bitcast_fusion.1), channel_id=1, source_target_pairs={{0,4},{4,8},{8,12},{12,16},{16,20},{20,24},{24,28},{28,0},{1,5},{5... | collective-permute-start | bytes 393224 | tf_op jit(solution)/shard_map/ppermute | solution.py:94
  19.3 8.1 %collective-permute-start.1 = (bf16[512,128]{0,1:T(8,128)(2,1)S(1)}, bf16[512,128]{0,1:T(8,128)(2,1)S(1)}, u32[]{:S(2)}, u32[]{:S(2)}) collective-permute-start(bf16[512,128]{0,1:T(8,128)(2,1)S(1)} %collective-permute-done), channel_id=1, source_target_pairs={{0,4},{4,8},{8,12},{12,16},{16,20},{20,24},{24,28},{28,0},{1,5},{5... | collective-permute-start | bytes 393224 | tf_op jit(solution)/shard_map/ppermute | solution.py:94
  27.5 8.4 %collective-permute-start.2 = (bf16[512,128]{0,1:T(8,128)(2,1)S(1)}, bf16[512,128]{0,1:T(8,128)(2,1)S(1)}, u32[]{:S(2)}, u32[]{:S(2)}) collective-permute-start(bf16[512,128]{0,1:T(8,128)(2,1)S(1)} %collective-permute-done.1), channel_id=1, source_target_pairs={{0,4},{4,8},{8,12},{12,16},{16,20},{20,24},{24,28},{28,0},{1,5},{5... | collective-permute-start | bytes 393224 | tf_op jit(solution)/shard_map/ppermute | solution.py:94
  35.8 7.8 %collective-permute-start.3 = (bf16[512,128]{0,1:T(8,128)(2,1)S(1)}, bf16[512,128]{0,1:T(8,128)(2,1)S(1)}, u32[]{:S(2)}, u32[]{:S(2)}) collective-permute-start(bf16[512,128]{0,1:T(8,128)(2,1)S(1)} %collective-permute-done.2), channel_id=1, source_target_pairs={{0,4},{4,8},{8,12},{12,16},{16,20},{20,24},{24,28},{28,0},{1,5},{5... | collective-permute-start | bytes 393224 | tf_op jit(solution)/shard_map/ppermute | solution.py:94
  43.6 10.5 %copy-start.6 = (bf16[512,128]{0,1:T(8,128)(2,1)}, bf16[512,128]{0,1:T(8,128)(2,1)S(1)}, u32[]{:S(2)}) copy-start(bf16[512,128]{0,1:T(8,128)(2,1)S(1)} %collective-permute-done.3) | copy-start | bytes 393220
  43.6 8.7 %collective-permute-start.4 = (bf16[512,128]{0,1:T(8,128)(2,1)S(1)}, bf16[512,128]{0,1:T(8,128)(2,1)S(1)}, u32[]{:S(2)}, u32[]{:S(2)}) collective-permute-start(bf16[512,128]{0,1:T(8,128)(2,1)S(1)} %collective-permute-done.3), channel_id=1, source_target_pairs={{0,4},{4,8},{8,12},{12,16},{16,20},{20,24},{24,28},{28,0},{1,5},{5... | collective-permute-start | bytes 393224 | tf_op jit(solution)/shard_map/ppermute | solution.py:94
  52.3 1.8 copy-start.8
  52.3 7.8 %collective-permute-start.5 = (bf16[512,128]{0,1:T(8,128)(2,1)S(1)}, bf16[512,128]{0,1:T(8,128)(2,1)}, u32[]{:S(2)}, u32[]{:S(2)}) collective-permute-start(bf16[512,128]{0,1:T(8,128)(2,1)S(1)} %collective-permute-done.4), channel_id=1, source_target_pairs={{0,4},{4,8},{8,12},{12,16},{16,20},{20,24},{24,28},{28,0},{1,5},{5... | collective-permute-start | bytes 393224 | tf_op jit(solution)/shard_map/ppermute | solution.py:94
  60.1 8.0 %collective-permute-start.6 = (bf16[512,128]{0,1:T(8,128)(2,1)}, bf16[512,128]{0,1:T(8,128)(2,1)}, u32[]{:S(2)}, u32[]{:S(2)}) collective-permute-start(bf16[512,128]{0,1:T(8,128)(2,1)} %collective-permute-done.5), channel_id=1, source_target_pairs={{0,4},{4,8},{8,12},{12,16},{16,20},{20,24},{24,28},{28,0},{1,5},{5... | collective-permute-start | bytes 393224 | tf_op jit(solution)/shard_map/ppermute | solution.py:94
  61.8 13.6 %copy-start.7 = (bf16[512,128]{0,1:T(8,128)(2,1)S(1)}, bf16[512,128]{0,1:T(8,128)(2,1)}, u32[]{:S(2)}) copy-start(bf16[512,128]{0,1:T(8,128)(2,1)} %copy-done.6) | copy-start | bytes 393220
  62.8 12.7 %copy-start.10 = (bf16[512,1,32]{0,2,1:T(8,128)(2,1)S(1)}, bf16[512,1,32]{0,2,1:T(8,128)(2,1)}, u32[]{:S(2)}) copy-start(bf16[512,1,32]{0,2,1:T(8,128)(2,1)} %copy-done.9) | copy-start | bytes 98308
  62.8 12.7 %copy-start.12 = (bf16[512,1,32]{0,2,1:T(8,128)(2,1)S(1)}, bf16[512,1,32]{0,2,1:T(8,128)(2,1)}, u32[]{:S(2)}) copy-start(bf16[512,1,32]{0,2,1:T(8,128)(2,1)} %copy-done.11) | copy-start | bytes 98308
  62.8 12.7 %copy-start.14 = (bf16[512,1,32]{0,2,1:T(8,128)(2,1)S(1)}, bf16[512,1,32]{0,2,1:T(8,128)(2,1)}, u32[]{:S(2)}) copy-start(bf16[512,1,32]{0,2,1:T(8,128)(2,1)} %copy-done.13) | copy-start | bytes 98308
  62.8 12.7 %copy-start.16 = (bf16[512,1,32]{0,2,1:T(8,128)(2,1)S(1)}, bf16[512,1,32]{0,2,1:T(8,128)(2,1)}, u32[]{:S(2)}) copy-start(bf16[512,1,32]{0,2,1:T(8,128)(2,1)} %copy-done.15) | copy-start | bytes 98308
  80.2 3.5 copy-start.1
  89.4 3.5 copy-start.1
  98.7 3.5 copy-start.1
  107.9 3.5 copy-start.1
  117.1 3.5 copy-start.1
  126.3 3.5 copy-start.1
  135.6 3.5 copy-start.1
  144.8 3.5 copy-start.1
  150.4 5.3 %copy-start.19 = (f32[512]{0:T(512)S(1)}, f32[512]{0:T(512)}, u32[]{:S(2)}) copy-start(f32[512]{0:T(512)} %fusion.25) | copy-start | bytes 6148
  151.2 13.5 %copy-start.5 = (bf16[128,2048]{1,0:T(8,128)(2,1)S(1)}, bf16[128,2048]{1,0:T(8,128)(2,1)}, u32[]{:S(2)}) copy-start(bf16[128,2048]{1,0:T(8,128)(2,1)} %param.21) | copy-start | bytes 1572868
  152.2 12.3 %all-to-all-start = ((bf16[4,128,512]{2,1,0:T(8,128)(2,1)}), bf16[4,128,512]{2,1,0:T(8,128)(2,1)S(1)}, u32[]{:S(2)}, u32[]{:S(2)}) async-start(bf16[4,128,512]{2,1,0:T(8,128)(2,1)} %all_to_all.20), calls=%async_computation | async-start | bytes 1048576 | tf_op jit(solution)/shard_map/all_to_all | solution.py:127
  164.7 4.8 %copy-start.17 = (f32[2048]{0:T(1024)S(1)}, f32[2048]{0:T(1024)}, u32[]{:S(2)}) copy-start(f32[2048]{0:T(1024)} %param.25) | copy-start | bytes 24580
  170.8 97.5 %copy-start.21 = (bf16[1,2048,256]{2,1,0:T(8,128)(2,1)S(1)}, bf16[1,2048,256]{2,1,0:T(8,128)(2,1)}, u32[]{:S(2)}) copy-start(bf16[1,2048,256]{2,1,0:T(8,128)(2,1)} %param.28) | copy-start | bytes 3145732
  266.3 2.0 copy-start.2
  279.7 3.8 copy-start.18
  279.7 4.0 %copy-start.4 = (bf16[2048,256]{1,0:T(8,128)(2,1)S(1)}, bf16[2048,256]{1,0:T(8,128)(2,1)}, u32[]{:S(2)}) copy-start(bf16[2048,256]{1,0:T(8,128)(2,1)} %param.31) | copy-start | bytes 3145732
  279.7 97.4 %all-to-all-start.2 = ((bf16[32,32,2048]{2,1,0:T(8,128)(2,1)}), bf16[32,32,2048]{2,1,0:T(8,128)(2,1)}, u32[]{:S(2)}, u32[]{:S(2)}) async-start(bf16[32,32,2048]{2,1,0:T(8,128)(2,1)} %convolution_convert_fusion), calls=%async_computation.2 | async-start | bytes 8388608 | tf_op jit(solution)/shard_map/all_to_all | solution.py:167
  389.2 3.9 copy-start.3
Sparse Core Ops, SparseCore 0:
  12.9 43.9 all-gather.1
